TPU v7x, 512 devices: a whole 4x8x8 slice. The times are simulated.
512 devices in a mesh: sp: 64 (over z, y), tp: 8 (over x, core).
Axes of the slice: x: 4, y: 8, z: 8, core: 2. Of those that a mesh axis runs over, the one named last changes fastest.
Arguments:
- resid: bfloat16 [24576, 2048], P('sp', 'tp'), may hold values from -40 to 40
- query_one: bfloat16 [24576, 1024], P('sp', 'tp'), may hold values from -64 to 64
- key_one: bfloat16 [24576, 1024], P('sp', 'tp'), may hold values from -64 to 64
- query_two: bfloat16 [24576, 1024], P('sp', 'tp'), may hold values from -64 to 64
- key_two: bfloat16 [24576, 1024], P('sp', 'tp'), may hold values from -64 to 64
- values: bfloat16 [24576, 2048], P('sp', 'tp'), may hold values from -6 to 6
- mix_lambda: float32 [8], P('tp'), may hold values from 0.3 to 0.8
- segments: int32 [24576], P('sp'), may hold values from 0 to 31, never falling along the last dimension, each value on 1 to 1536 neighbouring positions
- head_gain: float32 [256], replicated, may hold values from 0.1 to 1.9
- out_weight: bfloat16 [2048, 2048], P(None, 'tp'), may hold values from -0.125 to 0.125
- mixer_gain: float32 [2048], P('tp'), may hold values from 0.1 to 1.9
- gate_weight: bfloat16 [2048, 6144], P('sp', 'tp'), may hold values from -0.125 to 0.125
- up_weight: bfloat16 [2048, 6144], P('sp', 'tp'), may hold values from -0.125 to 0.125
- down_weight: bfloat16 [6144, 2048], P('tp', 'sp'), may hold values from -0.078125 to 0.078125
Outputs:
- layer_out: bfloat16 [24576, 2048], P('sp', 'tp')
Inputs may be any that keep to these rules, and one draw needn't show every extreme that they name: `segments`: numbers never fall along the sequence; each document has at most 1536 positions and one has exactly that many.
All inputs are finite; a program needn't handle non-finite values.
Results may differ from a plain program's by a relative error of at most 0.012.
Values may be sent and summed in bfloat16 or wider, within the bound.
A program may use at most 64 MiB of HBM per device.

v0:
```python
import jax
import jax.numpy as jnp
from jax import lax
from jax.sharding import PartitionSpec as P

HD = 128
VD = 256
REACH = 4


def rows_first(arrays, axis, dims):
    turned = [jnp.moveaxis(a, dim, 0) for a, dim in zip(arrays, dims)]
    widths = [t[0].size for t in turned]
    both = jnp.concatenate([t.reshape(-1, w) for t, w in zip(turned, widths)], axis=1)
    filled = lax.all_gather(both, axis, axis=0, tiled=True)
    pieces = jnp.split(filled, [sum(widths[:k]) for k in range(1, len(widths))], axis=1)
    return tuple(
        (
            jnp.moveaxis(b.reshape(-1, *t.shape[1:]), 0, dim)
            for b, t, dim in zip(pieces, turned, dims)
        )
    )


def shifted(value, axis, by):
    length = lax.axis_size(axis)
    pairs = [(i, i + by) for i in range(length) if 0 <= i + by < length]
    return lax.ppermute(value, axis, pairs)


def copy_for_each(value, axis):
    length = lax.axis_size(axis)
    return lax.all_to_all(
        jnp.broadcast_to(value[None], (length, *value.shape)), axis, 0, 0, tiled=True
    )


def joined_along(pieces, dim):
    pieces = jnp.moveaxis(pieces, 0, dim)
    dims = pieces.shape
    return pieces.reshape(*dims[:dim], dims[dim] * dims[dim + 1], *dims[dim + 2 :])


def gather_directly(value, axis, dim):
    pieces = copy_for_each(value, axis)
    return joined_along(pieces, dim)


def taken_together(value, axis):
    return copy_for_each(value, axis).sum(axis=0)


def split_up(value, dim, length):
    dims = value.shape
    pieces = value.reshape(*dims[:dim], length, dims[dim] // length, *dims[dim + 1 :])
    return jnp.moveaxis(pieces, dim, 0)


def sent_and_summed(value, axis, dim):
    length = lax.axis_size(axis)
    pieces = lax.all_to_all(split_up(value, dim, length), axis, 0, 0, tiled=True)
    return jnp.sum(pieces.astype(jnp.float32), axis=0)


def body(
    resid,
    query_one,
    key_one,
    query_two,
    key_two,
    values,
    mix_lambda,
    segments,
    head_gain,
    out_weight,
    mixer_gain,
    gate_weight,
    up_weight,
    down_weight,
):
    rows = query_one.shape[0]
    heads = mix_lambda.shape[0]
    gate_whole, up_whole, down_whole = rows_first(
        (gate_weight, up_weight, down_weight), "sp", (0, 0, 1)
    )
    position = lax.axis_index("sp")
    carried = (key_one, key_two, values, segments)
    earlier = [carried]
    for step in range(REACH):
        carried = shifted((carried[0], carried[1], carried[2], carried[3]), "sp", 1)
        earlier.insert(0, carried)
    width = (REACH + 1) * rows
    k_first = jnp.concatenate([piece[0] for piece in earlier], 0).reshape(width, heads, HD)
    k_second = jnp.concatenate([piece[1] for piece in earlier], 0).reshape(width, heads, HD)
    vals = jnp.concatenate([piece[2] for piece in earlier], 0).reshape(width, heads, VD)
    seg_key = jnp.concatenate([piece[3] for piece in earlier], 0)
    q_pos = position * rows + jnp.arange(rows, dtype=jnp.int32)
    k_pos = (position - REACH) * rows + jnp.arange(width, dtype=jnp.int32)
    allowed = (
        (seg_key[None, :] == segments[:, None])
        & (k_pos[None, :] <= q_pos[:, None])
        & (k_pos[None, :] >= 0)
    )

    def weights(query, keys):
        score = jnp.einsum(
            "qhd,khd->hqk", query.reshape(rows, heads, HD), keys, preferred_element_type=jnp.float32
        ) * HD ** (-0.5)
        score = jnp.where(allowed[None], score, -jnp.inf)
        score = score - jnp.max(score, axis=-1, keepdims=True)
        expo = jnp.exp(score)
        return (expo / jnp.sum(expo, axis=-1, keepdims=True)).astype(jnp.bfloat16)

    out_first = jnp.einsum(
        "hqk,khe->qhe", weights(query_one, k_first), vals, preferred_element_type=jnp.float32
    )
    out_second = jnp.einsum(
        "hqk,khe->qhe", weights(query_two, k_second), vals, preferred_element_type=jnp.float32
    )
    head_out = out_first - mix_lambda[None, :, None] * out_second
    meansq = jnp.mean(head_out * head_out, axis=-1, keepdims=True)
    attn_rows = (
        (head_out * lax.rsqrt(meansq + 1e-05) * head_gain)
        .reshape(rows, heads * VD)
        .astype(jnp.bfloat16)
    )
    projected = jnp.dot(
        gather_directly(attn_rows, "tp", 1), out_weight, preferred_element_type=jnp.float32
    )
    mid = (resid.astype(jnp.float32) + projected).astype(jnp.bfloat16)
    midf = mid.astype(jnp.float32)
    squares = taken_together(jnp.sum(midf * midf, axis=1), "tp")
    channels = mid.shape[1] * lax.axis_size("tp")
    normed = (midf * lax.rsqrt(squares / channels + 1e-06)[:, None] * mixer_gain).astype(
        jnp.bfloat16
    )
    whole_rows = gather_directly(normed, "tp", 1)
    gate = jnp.dot(whole_rows, gate_whole, preferred_element_type=jnp.float32)
    up = jnp.dot(whole_rows, up_whole, preferred_element_type=jnp.float32)
    hidden = (jax.nn.silu(gate) * up).astype(jnp.bfloat16)
    terms = jnp.dot(hidden, down_whole, preferred_element_type=jnp.float32)
    summed = sent_and_summed(terms.astype(jnp.bfloat16), "tp", 1)
    return (midf + summed).astype(jnp.bfloat16)


def solution(mesh):
    in_specs = (
        P("sp", "tp"),
        P("sp", "tp"),
        P("sp", "tp"),
        P("sp", "tp"),
        P("sp", "tp"),
        P("sp", "tp"),
        P("tp"),
        P("sp"),
        P(),
        P(None, "tp"),
        P("tp"),
        P("sp", "tp"),
        P("sp", "tp"),
        P("tp", "sp"),
    )
    out_specs = P("sp", "tp")
    return jax.shard_map(body, mesh=mesh, in_specs=in_specs, out_specs=out_specs, check_vma=False)
```

profile of v0, /device:TPU:256, one launch (start us, length us, event | category | flops | bytes accessed | tf_op | source)
XLA Modules:
  0.0 225.9 jit_solution(928105738986940786)
XLA Ops:
  8.2 3.5 %collective-permute-start.4 = (s32[384]{0:T(512)}, s32[384]{0:T(512)S(1)}, u32[]{:S(2)}, u32[]{:S(2)}) collective-permute-start(s32[384]{0:T(512)} %param.21), channel_id=1, source_target_pairs={{0,8},{8,16},{16,24},{24,32},{32,40},{40,48},{48,56},{56,64},{64,7... | collective-permute-start | bytes 4616 | tf_op jit(solution)/shard_map/ppermute | solution.py:28
  11.7 3.5 %collective-permute-start.12 = (bf16[384,128]{1,0:T(8,128)(2,1)}, bf16[384,128]{1,0:T(8,128)(2,1)S(1)}, u32[]{:S(2)}, u32[]{:S(2)}) collective-permute-start(bf16[384,128]{1,0:T(8,128)(2,1)} %param.18), channel_id=1, source_target_pairs={{0,8},{8,16},{16,24},{24,32},{32,40},{40,48},{48,56},{56,64},{64,7... | collective-permute-start | bytes 294920 | tf_op jit(solution)/shard_map/ppermute | solution.py:28
  15.2 3.5 %collective-permute-start = (bf16[384,256]{1,0:T(8,128)(2,1)}, bf16[384,256]{1,0:T(8,128)(2,1)S(1)}, u32[]{:S(2)}, u32[]{:S(2)}) collective-permute-start(bf16[384,256]{1,0:T(8,128)(2,1)} %param.19), channel_id=1, source_target_pairs={{0,8},{8,16},{16,24},{24,32},{32,40},{40,48},{48,56},{56,64},{64,7... | collective-permute-start | bytes 589832 | tf_op jit(solution)/shard_map/ppermute | solution.py:28
  18.7 4.7 %collective-permute-start.8 = (bf16[384,128]{1,0:T(8,128)(2,1)}, bf16[384,128]{1,0:T(8,128)(2,1)S(1)}, u32[]{:S(2)}, u32[]{:S(2)}) collective-permute-start(bf16[384,128]{1,0:T(8,128)(2,1)} %param.16), channel_id=1, source_target_pairs={{0,8},{8,16},{16,24},{24,32},{32,40},{40,48},{48,56},{56,64},{64,7... | collective-permute-start | bytes 294920 | tf_op jit(solution)/shard_map/ppermute | solution.py:28
  23.4 2.6 %collective-permute-start.5 = (s32[384]{0:T(512)S(1)}, s32[384]{0:T(512)S(1)}, u32[]{:S(2)}, u32[]{:S(2)}) collective-permute-start(s32[384]{0:T(512)S(1)} %collective-permute-done.4), channel_id=1, source_target_pairs={{0,8},{8,16},{16,24},{24,32},{32,40},{40,48},{48,56},{56,64},{64,7... | collective-permute-start | bytes 4616 | tf_op jit(solution)/shard_map/ppermute | solution.py:28
  26.0 6.2 %collective-permute-done.5 = s32[384]{0:T(512)S(1)} collective-permute-done((s32[384]{0:T(512)S(1)}, s32[384]{0:T(512)S(1)}, u32[]{:S(2)}, u32[]{:S(2)}) %collective-permute-start.5) | collective-permute-done | bytes 1568 | tf_op jit(solution)/shard_map/ppermute | solution.py:28
  32.2 1.9 collective-permute-start.6
  34.1 6.9 %collective-permute-done.6 = s32[384]{0:T(512)S(1)} collective-permute-done((s32[384]{0:T(512)S(1)}, s32[384]{0:T(512)S(1)}, u32[]{:S(2)}, u32[]{:S(2)}) %collective-permute-start.6) | collective-permute-done | bytes 1568 | tf_op jit(solution)/shard_map/ppermute | solution.py:28
  41.0 1.9 collective-permute-start.7
  43.6 6.3 %collective-permute-done.7 = s32[384]{0:T(512)S(1)} collective-permute-done((s32[384]{0:T(512)S(1)}, s32[384]{0:T(512)S(1)}, u32[]{:S(2)}, u32[]{:S(2)}) %collective-permute-start.7) | collective-permute-done | bytes 1568 | tf_op jit(solution)/shard_map/ppermute | solution.py:28
  49.8 1.9 collective-permute-start.13
  51.8 1.9 collective-permute-start.9
  53.7 5.9 %collective-permute-done.13 = bf16[384,128]{1,0:T(8,128)(2,1)S(1)} collective-permute-done((bf16[384,128]{1,0:T(8,128)(2,1)S(1)}, bf16[384,128]{1,0:T(8,128)(2,1)S(1)}, u32[]{:S(2)}, u32[]{:S(2)}) %collective-permute-start.13) | collective-permute-done | bytes 98336 | tf_op jit(solution)/shard_map/ppermute | solution.py:28
  59.7 1.9 collective-permute-start.14
  61.6 1.9 collective-permute-start.1
  63.5 1.9 collective-permute-start.10
  65.5 4.1 %collective-permute-done.14 = bf16[384,128]{1,0:T(8,128)(2,1)S(1)} collective-permute-done((bf16[384,128]{1,0:T(8,128)(2,1)S(1)}, bf16[384,128]{1,0:T(8,128)(2,1)S(1)}, u32[]{:S(2)}, u32[]{:S(2)}) %collective-permute-start.14) | collective-permute-done | bytes 98336 | tf_op jit(solution)/shard_map/ppermute | solution.py:28
  72.2 10.6 %collective-permute-done.10 = bf16[384,128]{1,0:T(8,128)(2,1)S(1)} collective-permute-done((bf16[384,128]{1,0:T(8,128)(2,1)S(1)}, bf16[384,128]{1,0:T(8,128)(2,1)S(1)}, u32[]{:S(2)}, u32[]{:S(2)}) %collective-permute-start.10) | collective-permute-done | bytes 98336 | tf_op jit(solution)/shard_map/ppermute | solution.py:28
  82.8 1.9 collective-permute-start.11
  84.8 1.9 collective-permute-start.2
  88.0 6.9 %collective-permute-done.11 = bf16[384,128]{1,0:T(8,128)(2,1)S(1)} collective-permute-done((bf16[384,128]{1,0:T(8,128)(2,1)S(1)}, bf16[384,128]{1,0:T(8,128)(2,1)S(1)}, u32[]{:S(2)}, u32[]{:S(2)}) %collective-permute-start.11) | collective-permute-done | bytes 98336 | tf_op jit(solution)/shard_map/ppermute | solution.py:28
  95.9 2.0 fusion.36
  99.5 3.8 %collective-permute-done.2 = bf16[384,256]{1,0:T(8,128)(2,1)S(1)} collective-permute-done((bf16[384,256]{1,0:T(8,128)(2,1)S(1)}, bf16[384,256]{1,0:T(8,128)(2,1)S(1)}, u32[]{:S(2)}, u32[]{:S(2)}) %collective-permute-start.2) | collective-permute-done | bytes 196640 | tf_op jit(solution)/shard_map/ppermute | solution.py:28
  103.3 1.9 collective-permute-start.3
  105.7 12.8 %collective-permute-done.3 = bf16[384,256]{1,0:T(8,128)(2,1)S(1)} collective-permute-done((bf16[384,256]{1,0:T(8,128)(2,1)S(1)}, bf16[384,256]{1,0:T(8,128)(2,1)S(1)}, u32[]{:S(2)}, u32[]{:S(2)}) %collective-permute-start.3) | collective-permute-done | bytes 196640 | tf_op jit(solution)/shard_map/ppermute | solution.py:28
  121.6 4.4 %all-to-all-start = ((bf16[8,384,256]{1,2,0:T(8,128)(2,1)}), bf16[8,384,256]{1,2,0:T(8,128)(2,1)S(1)}, u32[]{:S(2)}, u32[]{:S(2)}) async-start(bf16[8,384,256]{1,2,0:T(8,128)(2,1)} %broadcast_in_dim.12), calls=%async_computation | async-start | bytes 3145728 | tf_op jit(solution)/shard_map/all_to_all | solution.py:33
  126.2 21.4 %all-to-all-done = bf16[8,384,256]{1,2,0:T(8,128)(2,1)S(1)} async-done(((bf16[8,384,256]{1,2,0:T(8,128)(2,1)}), bf16[8,384,256]{1,2,0:T(8,128)(2,1)S(1)}, u32[]{:S(2)}, u32[]{:S(2)}) %all-to-all-start) | async-done | bytes 1572896 | tf_op jit(solution)/shard_map/all_to_all | solution.py:33
  148.4 7.7 %all_to_all.21 = f32[8,1,384]{2,1,0:T(1,128)S(1)} all-to-all(f32[8,1,384]{2,1,0:T(1,128)S(1)} %broadcast_in_dim.13), channel_id=1, replica_groups=mesh['sp'=64,'tp'=8] {'tp'}, dimensions={0} | all-to-all | bytes 24576 | tf_op jit(solution)/shard_map/all_to_all | solution.py:33
  156.4 24.0 %all_to_all.22 = bf16[8,384,256]{1,2,0:T(8,128)(2,1)S(1)} all-to-all(bf16[8,384,256]{1,2,0:T(8,128)(2,1)S(1)} %broadcast_in_dim.14), channel_id=1, replica_groups=mesh['sp'=64,'tp'=8] {'tp'}, dimensions={0} | all-to-all | bytes 3145728 | tf_op jit(solution)/shard_map/all_to_all | solution.py:33
  180.4 4.3 %fusion.4 = f32[384,768]{1,0:T(8,128)} fusion(bf16[384,2048]{0,1:T(8,128)(2,1)S(1)} %bitcast.42, bf16[2048,2304]{1,0:T(8,128)(2,1)} %all-gather.2.cloned.1.call-done), kind=kOutput, calls=%fused_computation.4 | convolution fusion | flops 1207959552 | bytes 5898240 | tf_op jit(solution)/shard_map/dot_general | solution.py:138
  184.8 7.5 %fusion.10 = bf16[384,2048]{1,0:T(8,128)(2,1)} fusion(bf16[2048,2304]{1,0:T(8,128)(2,1)} %all-gather.2.cloned.1.call-done, bf16[384,2048]{0,1:T(8,128)(2,1)S(1)} %bitcast.43, f32[384,768]{1,0:T(8,128)} %fusion.4), kind=kOutput, calls=%fused_computation.18 | convolution fusion | flops 2418475008 | bytes 10616832 | tf_op jit(solution)/shard_map/dot_general | solution.py:141
  193.8 24.0 %all_to_all.23 = bf16[8,384,256]{2,1,0:T(8,128)(2,1)S(1)} all-to-all(bf16[8,384,256]{2,1,0:T(8,128)(2,1)S(1)} %bitcast.40), channel_id=1, replica_groups=mesh['sp'=64,'tp'=8] {'tp'}, dimensions={0} | all-to-all | bytes 3145728 | tf_op jit(solution)/shard_map/all_to_all | solution.py:61
  (70 shorter events, 15.7 us)
Async XLA Ops:
  6.5 141.0 %copy-start = (bf16[2048,256]{1,0:T(8,128)(2,1)S(1)}, bf16[2048,256]{1,0:T(8,128)(2,1)}, u32[]{:S(2)}) copy-start(bf16[2048,256]{1,0:T(8,128)(2,1)} %param.23) | copy-start | bytes 3145732
  6.5 173.9 %all-gather.2.cloned.1.call-start = ((), (), s32[]{:S(2)}) async-start(), calls=%async_computation.4 | async-start | bytes 9584640 | tf_op jit(solution)/shard_map/all_gather | solution.py:15
  8.2 15.2 %collective-permute-start.4 = (s32[384]{0:T(512)}, s32[384]{0:T(512)S(1)}, u32[]{:S(2)}, u32[]{:S(2)}) collective-permute-start(s32[384]{0:T(512)} %param.21), channel_id=1, source_target_pairs={{0,8},{8,16},{16,24},{24,32},{32,40},{40,48},{48,56},{56,64},{64,7... | collective-permute-start | bytes 4616 | tf_op jit(solution)/shard_map/ppermute | solution.py:28
  11.7 38.2 %collective-permute-start.12 = (bf16[384,128]{1,0:T(8,128)(2,1)}, bf16[384,128]{1,0:T(8,128)(2,1)S(1)}, u32[]{:S(2)}, u32[]{:S(2)}) collective-permute-start(bf16[384,128]{1,0:T(8,128)(2,1)} %param.18), channel_id=1, source_target_pairs={{0,8},{8,16},{16,24},{24,32},{32,40},{40,48},{48,56},{56,64},{64,7... | collective-permute-start | bytes 294920 | tf_op jit(solution)/shard_map/ppermute | solution.py:28
  15.2 46.4 %collective-permute-start = (bf16[384,256]{1,0:T(8,128)(2,1)}, bf16[384,256]{1,0:T(8,128)(2,1)S(1)}, u32[]{:S(2)}, u32[]{:S(2)}) collective-permute-start(bf16[384,256]{1,0:T(8,128)(2,1)} %param.19), channel_id=1, source_target_pairs={{0,8},{8,16},{16,24},{24,32},{32,40},{40,48},{48,56},{56,64},{64,7... | collective-permute-start | bytes 589832 | tf_op jit(solution)/shard_map/ppermute | solution.py:28
  18.7 33.1 %collective-permute-start.8 = (bf16[384,128]{1,0:T(8,128)(2,1)}, bf16[384,128]{1,0:T(8,128)(2,1)S(1)}, u32[]{:S(2)}, u32[]{:S(2)}) collective-permute-start(bf16[384,128]{1,0:T(8,128)(2,1)} %param.16), channel_id=1, source_target_pairs={{0,8},{8,16},{16,24},{24,32},{32,40},{40,48},{48,56},{56,64},{64,7... | collective-permute-start | bytes 294920 | tf_op jit(solution)/shard_map/ppermute | solution.py:28
  23.4 8.8 %collective-permute-start.5 = (s32[384]{0:T(512)S(1)}, s32[384]{0:T(512)S(1)}, u32[]{:S(2)}, u32[]{:S(2)}) collective-permute-start(s32[384]{0:T(512)S(1)} %collective-permute-done.4), channel_id=1, source_target_pairs={{0,8},{8,16},{16,24},{24,32},{32,40},{40,48},{48,56},{56,64},{64,7... | collective-permute-start | bytes 4616 | tf_op jit(solution)/shard_map/ppermute | solution.py:28
  32.2 8.8 %collective-permute-start.6 = (s32[384]{0:T(512)S(1)}, s32[384]{0:T(512)S(1)}, u32[]{:S(2)}, u32[]{:S(2)}) collective-permute-start(s32[384]{0:T(512)S(1)} %collective-permute-done.5), channel_id=1, source_target_pairs={{0,8},{8,16},{16,24},{24,32},{32,40},{40,48},{48,56},{56,64},{64,7... | collective-permute-start | bytes 4616 | tf_op jit(solution)/shard_map/ppermute | solution.py:28
  41.0 8.8 %collective-permute-start.7 = (s32[384]{0:T(512)S(1)}, s32[384]{0:T(512)S(1)}, u32[]{:S(2)}, u32[]{:S(2)}) collective-permute-start(s32[384]{0:T(512)S(1)} %collective-permute-done.6), channel_id=1, source_target_pairs={{0,8},{8,16},{16,24},{24,32},{32,40},{40,48},{48,56},{56,64},{64,7... | collective-permute-start | bytes 4616 | tf_op jit(solution)/shard_map/ppermute | solution.py:28
  49.8 9.8 %collective-permute-start.13 = (bf16[384,128]{1,0:T(8,128)(2,1)S(1)}, bf16[384,128]{1,0:T(8,128)(2,1)S(1)}, u32[]{:S(2)}, u32[]{:S(2)}) collective-permute-start(bf16[384,128]{1,0:T(8,128)(2,1)S(1)} %collective-permute-done.12), channel_id=1, source_target_pairs={{0,8},{8,16},{16,24},{24,32},{32,40},{40,48},{48,56},{56,64},{64,7... | collective-permute-start | bytes 294920 | tf_op jit(solution)/shard_map/ppermute | solution.py:28
  51.8 11.8 %collective-permute-start.9 = (bf16[384,128]{1,0:T(8,128)(2,1)S(1)}, bf16[384,128]{1,0:T(8,128)(2,1)S(1)}, u32[]{:S(2)}, u32[]{:S(2)}) collective-permute-start(bf16[384,128]{1,0:T(8,128)(2,1)S(1)} %collective-permute-done.8), channel_id=1, source_target_pairs={{0,8},{8,16},{16,24},{24,32},{32,40},{40,48},{48,56},{56,64},{64,7... | collective-permute-start | bytes 294920 | tf_op jit(solution)/shard_map/ppermute | solution.py:28
  59.7 9.9 %collective-permute-start.14 = (bf16[384,128]{1,0:T(8,128)(2,1)S(1)}, bf16[384,128]{1,0:T(8,128)(2,1)S(1)}, u32[]{:S(2)}, u32[]{:S(2)}) collective-permute-start(bf16[384,128]{1,0:T(8,128)(2,1)S(1)} %collective-permute-done.13), channel_id=1, source_target_pairs={{0,8},{8,16},{16,24},{24,32},{32,40},{40,48},{48,56},{56,64},{64,7... | collective-permute-start | bytes 294920 | tf_op jit(solution)/shard_map/ppermute | solution.py:28
  61.6 23.2 %collective-permute-start.1 = (bf16[384,256]{1,0:T(8,128)(2,1)S(1)}, bf16[384,256]{1,0:T(8,128)(2,1)S(1)}, u32[]{:S(2)}, u32[]{:S(2)}) collective-permute-start(bf16[384,256]{1,0:T(8,128)(2,1)S(1)} %collective-permute-done), channel_id=1, source_target_pairs={{0,8},{8,16},{16,24},{24,32},{32,40},{40,48},{48,56},{56,64},{64,7... | collective-permute-start | bytes 589832 | tf_op jit(solution)/shard_map/ppermute | solution.py:28
  63.5 19.3 %collective-permute-start.10 = (bf16[384,128]{1,0:T(8,128)(2,1)S(1)}, bf16[384,128]{1,0:T(8,128)(2,1)S(1)}, u32[]{:S(2)}, u32[]{:S(2)}) collective-permute-start(bf16[384,128]{1,0:T(8,128)(2,1)S(1)} %collective-permute-done.9), channel_id=1, source_target_pairs={{0,8},{8,16},{16,24},{24,32},{32,40},{40,48},{48,56},{56,64},{64,7... | collective-permute-start | bytes 294920 | tf_op jit(solution)/shard_map/ppermute | solution.py:28
  69.6 17.4 %collective-permute-start.15 = (bf16[384,128]{1,0:T(8,128)(2,1)S(1)}, bf16[384,128]{1,0:T(8,128)(2,1)S(1)}, u32[]{:S(2)}, u32[]{:S(2)}) collective-permute-start(bf16[384,128]{1,0:T(8,128)(2,1)S(1)} %collective-permute-done.14), channel_id=1, source_target_pairs={{0,8},{8,16},{16,24},{24,32},{32,40},{40,48},{48,56},{56,64},{64,7... | collective-permute-start | bytes 294920 | tf_op jit(solution)/shard_map/ppermute | solution.py:28
  82.8 12.1 %collective-permute-start.11 = (bf16[384,128]{1,0:T(8,128)(2,1)S(1)}, bf16[384,128]{1,0:T(8,128)(2,1)S(1)}, u32[]{:S(2)}, u32[]{:S(2)}) collective-permute-start(bf16[384,128]{1,0:T(8,128)(2,1)S(1)} %collective-permute-done.10), channel_id=1, source_target_pairs={{0,8},{8,16},{16,24},{24,32},{32,40},{40,48},{48,56},{56,64},{64,7... | collective-permute-start | bytes 294920 | tf_op jit(solution)/shard_map/ppermute | solution.py:28
  84.8 18.5 %collective-permute-start.2 = (bf16[384,256]{1,0:T(8,128)(2,1)S(1)}, bf16[384,256]{1,0:T(8,128)(2,1)S(1)}, u32[]{:S(2)}, u32[]{:S(2)}) collective-permute-start(bf16[384,256]{1,0:T(8,128)(2,1)S(1)} %collective-permute-done.1), channel_id=1, source_target_pairs={{0,8},{8,16},{16,24},{24,32},{32,40},{40,48},{48,56},{56,64},{64,7... | collective-permute-start | bytes 589832 | tf_op jit(solution)/shard_map/ppermute | solution.py:28
  95.9 2.0 copy-start.3
  95.9 2.0 copy-start.6
  99.5 19.1 %copy-start.1 = (bf16[384,256]{1,0:T(8,128)(2,1)S(1)}, bf16[384,256]{1,0:T(8,128)(2,1)}, u32[]{:S(2)}) copy-start(bf16[384,256]{1,0:T(8,128)(2,1)} %param.19) | copy-start | bytes 589828
  103.3 15.2 %collective-permute-start.3 = (bf16[384,256]{1,0:T(8,128)(2,1)S(1)}, bf16[384,256]{1,0:T(8,128)(2,1)S(1)}, u32[]{:S(2)}, u32[]{:S(2)}) collective-permute-start(bf16[384,256]{1,0:T(8,128)(2,1)S(1)} %collective-permute-done.2), channel_id=1, source_target_pairs={{0,8},{8,16},{16,24},{24,32},{32,40},{40,48},{48,56},{56,64},{64,7... | collective-permute-start | bytes 589832 | tf_op jit(solution)/shard_map/ppermute | solution.py:28
  119.4 0.8 copy-start.4
  120.2 5.8 %copy-start.2 = (bf16[384,256]{1,0:T(8,128)(2,1)S(1)}, bf16[384,256]{1,0:T(8,128)(2,1)}, u32[]{:S(2)}) copy-start(bf16[384,256]{1,0:T(8,128)(2,1)} %param.14) | copy-start | bytes 589828
  121.6 34.5 %copy-start.5 = (f32[256]{0:T(256)S(1)}, f32[256]{0:T(256)}, u32[]{:S(2)}) copy-start(f32[256]{0:T(256)} %param.24) | copy-start | bytes 3076
  121.6 25.9 %all-to-all-start = ((bf16[8,384,256]{1,2,0:T(8,128)(2,1)}), bf16[8,384,256]{1,2,0:T(8,128)(2,1)S(1)}, u32[]{:S(2)}, u32[]{:S(2)}) async-start(bf16[8,384,256]{1,2,0:T(8,128)(2,1)} %broadcast_in_dim.12), calls=%async_computation | async-start | bytes 3145728 | tf_op jit(solution)/shard_map/all_to_all | solution.py:33
Sparse Core Ops, SparseCore 0:
  10.3 119.3 all-gather.1
where the time goes:
time: 227 us; the launch traced here: 226 us
  waiting for transfers between devices  85.2 us (38%)
  blocking collectives  55.7 us (25%)
  starting transfers between devices  43.2 us (19%)
  matrix products  17.2 us (8%)
  between operations  14.5 us (6%)
  local copies, waits for them, and re-layouts  6.85 us (3%)
  other arithmetic  3.17 us (1%)
    ppermute x16, waiting for transfers between devices, shifted(): return lax.ppermute(value, axis, pairs)  63.8 us
    ppermute x16, starting transfers between devices, shifted(): return lax.ppermute(value, axis, pairs)  38.8 us
    all_to_all x2, blocking collectives, copy_for_each(): lax.all_to_all(jnp.broadcast_to(value[None], (length, *value.shape)), axi...  31.7 us
    all_to_all x1, blocking collectives, sent_and_summed(): lax.all_to_all(split_up(value, dim, length), axis, 0, 0, tiled=True)  24 us
    all_to_all x1, waiting for transfers between devices, copy_for_each(): lax.all_to_all(jnp.broadcast_to(value[None], (length, *value.shape)), axi...  21.4 us
    dot_general x1, matrix products, body(): terms = jnp.dot(hidden, down_whole, preferred_element_type=jnp.float32)  7.54 us
  transfers between devices with their start and end apart: 18, of which 11 were waited for; matrix products, arithmetic and copies ran while one was open for 5% of the time, Pallas kernels for 0%

commit v1 on v0

v1 whole, which is shorter than its diff:
```python
import functools

import jax
import jax.numpy as jnp
from jax import lax
from jax.experimental import pallas as pl
from jax.experimental.pallas import tpu as pltpu
from jax.sharding import PartitionSpec as P

MESH = pl.DeviceIdType.MESH
BF, F32 = jnp.bfloat16, jnp.float32
ROWS, HALF, HD, VD = 384, 192, 128, 256
REACH = 4
BW, AW, GU = 1280, 1024, 768
YM, YP, ZM, ZP = 5, 2, 4, 3
NT = (((1,), (1,)), ((), ()))


def dot(a, b):
    return jnp.dot(a, b, preferred_element_type=F32)


def dot_nt(a, b):
    return lax.dot_general(a, b, NT, preferred_element_type=F32)


def kernel(
    q1_h, q2_h, k1_h, k2_h, v_h, resid_h, wout_h, gate_h, up_h, down_h, seg_h, hg, mg, lam,
    out_ref,
    q1, q2, resid, wout, dwn, kbuf, vbuf, gbuf, bbuf, abuf, segq, gains, mref, lref, oacc,
    heads, mids, xn, hid, pown, psend, precv, stage, rhalf, rfull,
    loc, kv_s, kv_r, b1m_s, b1m_r, b1p_s, b1p_r, a1m_s, a1m_r, a1p_s, a1p_r,
    b20_s, b20_r, a20_s, a20_r, b2m_s, b2m_r, b2p_s, b2p_r, a2m_s, a2m_r, a2p_s, a2p_r,
    xg_s, xg_r, d_s, d_r, rs_s, rs_r,
):
    s, t = lax.axis_index("sp"), lax.axis_index("tp")
    z, y = lax.div(s, 8), lax.rem(s, 8)
    x, c = lax.div(t, 2), lax.rem(t, 2)
    o = 1 - c

    def ring(i, by, n):
        return lax.rem(i + (by % n), n)

    yp, ym = {"sp": z * 8 + ring(y, 1, 8)}, {"sp": z * 8 + ring(y, -1, 8)}
    zp, zm = {"sp": ring(z, 1, 8) * 8 + y}, {"sp": ring(z, -1, 8) * 8 + y}
    kp, km = {"sp": ring(s, 1, 64)}, {"sp": ring(s, -1, 64)}
    xp, xm = {"tp": ring(x, 1, 4) * 2 + c}, {"tp": ring(x, -1, 4) * 2 + c}
    pc = {"tp": x * 2 + o}

    barrier = pltpu.get_barrier_semaphore()
    for dev in (yp, ym, zp, zm, kp, km, xp, xm, pc):
        pl.semaphore_signal(barrier, inc=1, device_id=dev, device_id_type=MESH)

    loads = [
        (k1_h, kbuf.at[0, :, 0:HD]),
        (k2_h, kbuf.at[0, :, HD : 2 * HD]),
        (v_h, vbuf.at[0]),
        (gate_h, bbuf.at[z, y, :, 0:GU]),
        (up_h, abuf.at[z, y, :, 0:GU]),
        (seg_h, gbuf.at[0]),
        (down_h, dwn),
        (q1_h, q1),
        (q2_h, q2),
        (resid_h, resid),
        (wout_h, wout),
    ]
    loads = [pltpu.make_async_copy(a, b, loc.at[i]) for i, (a, b) in enumerate(loads)]
    for i in (6, 3, 4, 0, 1, 2, 5, 7, 8, 9, 10):
        loads[i].start()

    gains[t] = jnp.broadcast_to(mg[...], (16, VD))
    loads[6].wait()
    eye = (
        lax.broadcasted_iota(jnp.int32, (32, 32), 0) == lax.broadcasted_iota(jnp.int32, (32, 32), 1)
    )
    turned = dot_nt(jnp.where(eye, 1.0, 0.0).astype(BF), dwn[...]).astype(BF)
    bbuf[z, y, :, GU:BW] = turned[:, : BW - GU]
    abuf[z, y, :, GU:AW] = turned[:, BW - GU :]
    for i in (3, 4, 0, 1, 2, 5):
        loads[i].wait()
    pl.semaphore_wait(barrier, 9)

    pending = []

    def copy(src, dst, ss, rs, dev):
        return pltpu.make_async_remote_copy(
            src_ref=src, dst_ref=dst, send_sem=ss, recv_sem=rs, device_id=dev, device_id_type=MESH
        )

    def send(src, dst, ss, rs, dev):
        one = copy(src, dst, ss, rs, dev)
        one.start()
        pending.append(one)

    def got(ref, ss, rs):
        copy(ref, ref, ss, rs, pc).wait_recv()

    def b_first(which, hop):
        dev, ss, rs, last, step = (
            (ym, b1m_s, b1m_r, YM, 1) if which else (yp, b1p_s, b1p_r, YP, -1)
        )
        shard = y if hop < 0 else ring(y, step * (hop + 1), 8)
        ref = bbuf.at[z, shard]
        if hop >= 0:
            got(ref, ss.at[hop], rs.at[hop])
        if hop + 1 < last:
            send(ref, ref, ss.at[hop + 1], rs.at[hop + 1], dev)
        if hop >= 0 or which:
            for k, far in enumerate((zm, zp)):
                copy(ref, ref, b20_s.at[k], b20_r.at[k], far).start()

    def a_first(which, hop):
        dev, ss, rs, last, step = (
            (zm, a1m_s, a1m_r, ZM, 1) if which else (zp, a1p_s, a1p_r, ZP, -1)
        )
        shard = z if hop < 0 else ring(z, step * (hop + 1), 8)
        ref = abuf.at[shard, y]
        if hop >= 0:
            got(ref, ss.at[hop], rs.at[hop])
        if hop + 1 < last:
            send(ref, ref, ss.at[hop + 1], rs.at[hop + 1], dev)
        if hop >= 0 or which:
            copy(ref, ref, a20_s, a20_r, ym).start()

    def b_part(row, k):
        return bbuf.at[row, :, :, 0:GU] if k == 0 else bbuf.at[row, :, :, GU:BW]

    def a_part(col, k):
        return abuf.at[:, col, :, 0:GU] if k == 0 else abuf.at[:, col, :, GU:AW]

    def b_second(which, hop, part):
        dev, ss, rs, last, step = (
            (zm, b2m_s, b2m_r, ZM, 1) if which else (zp, b2p_s, b2p_r, ZP, -1)
        )
        row = ring(z, step * (hop + 1), 8)
        if hop == 0:
            k = 0 if which else 1
            got(bbuf.at[row], b20_s.at[k], b20_r.at[k])
        else:
            got(b_part(row, part), ss.at[hop, part], rs.at[hop, part])
        for k in (0, 1) if hop == 0 else (part,):
            if hop + 1 < last:
                ref = b_part(row, k)
                send(ref, ref, ss.at[hop + 1, k], rs.at[hop + 1, k], dev)

    def a_second(which, hop, part):
        dev, ss, rs, last, step = (
            (ym, a2m_s, a2m_r, YM, 1) if which else (yp, a2p_s, a2p_r, YP, -1)
        )
        col = ring(y, step * (hop + 1), 8)
        if hop == 0 and which:
            got(abuf.at[:, col], a20_s, a20_r)
        else:
            got(a_part(col, part), ss.at[hop, part], rs.at[hop, part])
        for k in (0, 1) if hop == 0 and which else (part,):
            if hop + 1 < last:
                ref = a_part(col, k)
                send(ref, ref, ss.at[hop + 1, k], rs.at[hop + 1, k], dev)

    def a_own():
        for k in (0, 1):
            ref = a_part(y, k)
            send(ref, ref, a2p_s.at[0, k], a2p_r.at[0, k], yp)

    def kv(slot, part):
        bufs = ((0, kbuf), (2, gbuf)) if part == 0 else ((1, vbuf),)
        for i, buf in bufs:
            if slot > 0:
                got(buf.at[slot], kv_s.at[i, slot], kv_r.at[i, slot])
            if slot < REACH:
                send(buf.at[slot], buf.at[slot + 1], kv_s.at[i, slot + 1], kv_r.at[i, slot + 1], kp)

    def attend(k):
        ids = gbuf[k].astype(F32) + jnp.where(s >= k, 0.0, 1000.0)

        def chunk(i, carry):
            rows = pl.ds(pl.multiple_of(i * 128, 128), 128)
            same = segq[rows, 0:1] == ids
            if k == 0:
                qpos = i * 128 + lax.broadcasted_iota(jnp.int32, (128, ROWS), 0)
                same = same & (lax.broadcasted_iota(jnp.int32, (128, ROWS), 1) <= qpos)
            for m, q in enumerate((q1, q2)):
                score = dot_nt(q[rows, :], kbuf[k, :, m * HD : (m + 1) * HD])
                score = jnp.where(same, score * (HD**-0.5 * 1.4426950408889634), -jnp.inf)
                top = jnp.max(score, axis=1, keepdims=True)
                if k > 0:
                    before = mref[m, rows, 0:1]
                    top = jnp.maximum(top, before)
                expo = jnp.exp2(score - top)
                total = jnp.sum(expo, axis=1, keepdims=True)
                value = dot(expo.astype(BF), vbuf[k])
                if k > 0:
                    scale = jnp.exp2(before - top)
                    total = total + scale * lref[m, rows, 0:1]
                    value = value + scale * oacc[m, rows, :]
                mref[m, rows, :] = jnp.broadcast_to(top, (128, 128))
                lref[m, rows, :] = jnp.broadcast_to(total, (128, 128))
                oacc[m, rows, :] = value
            return carry

        lax.fori_loop(0, 3, chunk, 0)

    def finish_heads():
        def chunk(i, carry):
            rows = pl.ds(pl.multiple_of(i * 64, 64), 64)
            head = oacc[0, rows, :] / lref[0, rows, 0:1]
            head = head - lam[0] * (oacc[1, rows, :] / lref[1, rows, 0:1])
            meansq = jnp.mean(head * head, axis=1, keepdims=True)
            heads[t, rows, :] = (head * lax.rsqrt(meansq + 1e-05) * hg[...]).astype(BF)
            return carry

        lax.fori_loop(0, 6, chunk, 0)

    def slot_of(by, core):
        return ring(x, by, 4) * 2 + core

    def x_gather(buf, g):
        n = buf.shape[1]
        low, high = pl.ds(0, n // 2), pl.ds(n // 2, n // 2)

        def go(ref, i, dev):
            send(ref, ref, xg_s.at[g, i], xg_r.at[g, i], dev)

        def come(ref, i):
            got(ref, xg_s.at[g, i], xg_r.at[g, i])

        def own():
            go(buf.at[t], 0, xp)
            go(buf.at[t], 1, xm)
            go(buf.at[t], 4, pc)

        def near():
            a, b = buf.at[slot_of(-1, c)], buf.at[slot_of(1, c)]
            come(a, 0)
            go(buf.at[slot_of(-1, c), low], 2, xp)
            go(a, 5, pc)
            come(b, 1)
            go(buf.at[slot_of(1, c), high], 3, xm)
            go(b, 6, pc)

        def far():
            for i, part in ((2, low), (3, high)):
                ref = buf.at[slot_of(2, c), part]
                come(ref, i)
                go(ref, i + 5, pc)

        def across():
            come(buf.at[slot_of(0, o)], 4)
            come(buf.at[slot_of(-1, o)], 5)
            come(buf.at[slot_of(1, o)], 6)

        def across_far():
            for i, part in ((2, low), (3, high)):
                come(buf.at[slot_of(2, o), part], i + 5)

        return own, near, far, across, across_far

    gain_g = x_gather(gains, 0)
    head_g = x_gather(heads, 1)
    mid_g = x_gather(mids, 2)

    def project(slots, first):
        total = None if first else oacc[0]
        for by, core in slots:
            i = slot_of(by, core)
            w = wout[pl.ds(pl.multiple_of(i * VD, VD), VD), :]
            part = dot(heads[i], w)
            total = part if total is None else total + part
        oacc[0] = total

    def project_near():
        project(((0, c), (-1, c), (1, c), (0, o), (-1, o), (1, o)), True)

    def project_far():
        project(((2, c), (2, o)), False)
        mids[t] = (resid[...].astype(F32) + oacc[0]).astype(BF)

    def normalise():
        def chunk(i, carry):
            rows = pl.ds(pl.multiple_of(i * 32, 32), 32)
            mid = [mids[j, rows, :].astype(F32) for j in range(8)]
            squares = sum([m * m for m in mid])
            meansq = jnp.sum(squares, axis=1, keepdims=True) * (1.0 / (8 * VD))
            scale = lax.rsqrt(meansq + 1e-06)
            for j in range(8):
                gain = gains[j][0:1, :]
                xn[rows, j * VD : (j + 1) * VD] = (mid[j] * scale * gain).astype(BF)
            return carry

        lax.fori_loop(0, 12, chunk, 0)

    def hidden():
        def tile(i, carry):
            cols = pl.ds(pl.multiple_of(i * 256, 256), 256)
            gate = dot(xn[...], bbuf[:, :, :, cols].reshape(2048, 256))
            up = dot(xn[...], abuf[:, :, :, cols].reshape(2048, 256))
            hid[:, cols] = (gate / (1.0 + jnp.exp(-gate)) * up).astype(BF)
            return carry

        lax.fori_loop(0, 3, tile, 0)

    def terms(i):
        one = dot_nt(hid[:, 0 : BW - GU], bbuf[i, :, :, GU:BW].reshape(256, BW - GU))
        return one + dot_nt(hid[:, BW - GU :], abuf[i, :, :, GU:AW].reshape(256, AW - GU))

    events = []

    def at(time, what, *args):
        events.append((time, len(events), what, args))

    for hop in range(YM):
        at(3.5 * (hop + 1), b_first, True, hop)
        if hop < YP:
            at(3.5 * (hop + 1) + 0.1, b_first, False, hop)
        if hop < ZM:
            at(3.5 * (hop + 1) + 0.2, a_first, True, hop)
        if hop < ZP:
            at(3.5 * (hop + 1) + 0.3, a_first, False, hop)
    at(2.0, gain_g[0])
    at(7.5, gain_g[1])
    at(11.0, gain_g[2])
    at(11.1, gain_g[3])
    at(14.5, gain_g[4])
    at(2.1, attend, 0)
    for slot, (tk, tv) in enumerate(((7.7, 12.0), (18.0, 22.0), (26.3, 30.5), (34.7, 39.0))):
        at(tk, kv, slot + 1, 0)
        at(tv, kv, slot + 1, 1)
        at(tv + 0.1, attend, slot + 1)
    at(30.6, a_own)
    for which, times in ((True, ((22, 22), (32.5, 38), (46.5, 52.5), (60.5, 66))),
                         (False, ((22.1, 22.1), (32.6, 38.1), (46.6, 52.6)))):
        for hop, pair in enumerate(times):
            at(pair[0], b_second, which, hop, 0)
            if hop:
                at(pair[1], b_second, which, hop, 1)
    for which, times in ((True, ((20, 20), (30.7, 33.7), (42, 45), (53, 56), (60.4, 67))),
                         (False, ((48, 51), (60.3, 65)))):
        for hop, pair in enumerate(times):
            at(pair[0], a_second, which, hop, 0)
            if hop or not which:
                at(pair[1], a_second, which, hop, 1)
    at(40.0, finish_heads)
    at(40.1, head_g[0])
    at(46.0, head_g[1])
    at(47.0, head_g[3])
    at(47.1, project_near)
    at(48.5, head_g[2])
    at(49.5, head_g[4])
    at(49.6, project_far)
    at(49.7, mid_g[0])
    at(55.5, mid_g[1])
    at(58.0, mid_g[2])
    at(59.0, mid_g[3])
    at(59.1, mid_g[4])
    at(59.2, normalise)
    at(61.0, hidden)

    b_first(True, -1)
    b_first(False, -1)
    a_first(True, -1)
    a_first(False, -1)
    kv(0, 0)
    kv(0, 1)
    for i in (7, 8):
        loads[i].wait()
    ids = jnp.broadcast_to(gbuf[0].astype(F32), (128, ROWS))
    segq[...] = ids.T
    for i in (9, 10):
        loads[i].wait()
    for _, _, what, args in sorted(events, key=lambda e: e[:2]):
        what(*args)

    chips = (2, 1, -1, 0)
    for i, by in enumerate(chips):
        psend[i] = terms(slot_of(by, o)).astype(BF)
        send(psend.at[i], precv.at[i], d_s.at[i], d_r.at[i], pc)
        pown[i] = terms(slot_of(by, c))
    low, high = pl.ds(0, HALF), pl.ds(HALF, HALF)

    def pair(i, part):
        return pown[i, part, :] + precv[i, part, :].astype(F32)

    got(precv.at[0], d_s.at[0], d_r.at[0])
    stage[0, low, :] = pair(0, low).astype(BF)
    send(stage.at[0, low], rhalf.at[0], rs_s.at[0], rs_r.at[0], xp)
    stage[0, high, :] = pair(0, high).astype(BF)
    send(stage.at[0, high], rhalf.at[1], rs_s.at[1], rs_r.at[1], xm)
    got(precv.at[1], d_s.at[1], d_r.at[1])
    stage[1, high, :] = pair(1, high).astype(BF)
    send(stage.at[1, high], rfull.at[0, high], rs_s.at[2], rs_r.at[2], xp)
    got(precv.at[2], d_s.at[2], d_r.at[2])
    stage[2, low, :] = pair(2, low).astype(BF)
    send(stage.at[2, low], rfull.at[1, low], rs_s.at[3], rs_r.at[3], xm)
    got(rhalf.at[0], rs_s.at[0], rs_r.at[0])
    stage[1, low, :] = (pair(1, low) + rhalf[0].astype(F32)).astype(BF)
    send(stage.at[1, low], rfull.at[0, low], rs_s.at[4], rs_r.at[4], xp)
    got(rhalf.at[1], rs_s.at[1], rs_r.at[1])
    stage[2, high, :] = (pair(2, high) + rhalf[1].astype(F32)).astype(BF)
    send(stage.at[2, high], rfull.at[1, high], rs_s.at[5], rs_r.at[5], xm)
    got(precv.at[3], d_s.at[3], d_r.at[3])
    pown[3] = pown[3] + precv[3].astype(F32) + mids[t].astype(F32)
    got(rfull.at[0, high], rs_s.at[2], rs_r.at[2])
    got(rfull.at[1, low], rs_s.at[3], rs_r.at[3])
    got(rfull.at[0, low], rs_s.at[4], rs_r.at[4])
    got(rfull.at[1, high], rs_s.at[5], rs_r.at[5])
    out_ref[...] = (pown[3] + rfull[0].astype(F32) + rfull[1].astype(F32)).astype(BF)

    for one in pending:
        one.wait_send()
    copy(bbuf.at[z], bbuf.at[z], b20_s.at[0], b20_r.at[0], zm).wait_send()
    copy(bbuf.at[z], bbuf.at[z], b20_s.at[1], b20_r.at[1], zp).wait_send()
    copy(abuf.at[:, y], abuf.at[:, y], a20_s, a20_r, ym).wait_send()


def body(
    resid, query_one, key_one, query_two, key_two, values, mix_lambda, segments, head_gain,
    out_weight, mixer_gain, gate_weight, up_weight, down_weight,
):
    hbm = pl.BlockSpec(memory_space=pltpu.HBM)
    vmem = pl.BlockSpec(memory_space=pltpu.VMEM)
    dma = pltpu.SemaphoreType.DMA
    scratch = [
        pltpu.VMEM((ROWS, HD), BF), pltpu.VMEM((ROWS, HD), BF), pltpu.VMEM((ROWS, VD), BF),
        pltpu.VMEM((2048, VD), BF), pltpu.VMEM((768, 32), BF),
        pltpu.VMEM((5, ROWS, 2 * HD), BF), pltpu.VMEM((5, ROWS, VD), BF),
        pltpu.VMEM((5, 1, ROWS), jnp.int32),
        pltpu.VMEM((8, 8, 32, BW), BF), pltpu.VMEM((8, 8, 32, AW), BF),
        pltpu.VMEM((ROWS, 128), F32), pltpu.VMEM((8, 16, VD), F32),
        pltpu.VMEM((2, ROWS, 128), F32), pltpu.VMEM((2, ROWS, 128), F32),
        pltpu.VMEM((2, ROWS, VD), F32),
        pltpu.VMEM((8, ROWS, VD), BF), pltpu.VMEM((8, ROWS, VD), BF),
        pltpu.VMEM((ROWS, 2048), BF), pltpu.VMEM((ROWS, 768), BF),
        pltpu.VMEM((4, ROWS, VD), F32), pltpu.VMEM((4, ROWS, VD), BF),
        pltpu.VMEM((4, ROWS, VD), BF), pltpu.VMEM((3, ROWS, VD), BF),
        pltpu.VMEM((2, HALF, VD), BF), pltpu.VMEM((2, ROWS, VD), BF),
        dma((11,)), dma((3, 5)), dma((3, 5)),
        dma((YM,)), dma((YM,)), dma((YP,)), dma((YP,)),
        dma((ZM,)), dma((ZM,)), dma((ZP,)), dma((ZP,)),
        dma((2,)), dma((2,)), dma, dma,
        dma((ZM, 2)), dma((ZM, 2)), dma((ZP, 2)), dma((ZP, 2)),
        dma((YM, 2)), dma((YM, 2)), dma((YP, 2)), dma((YP, 2)),
        dma((3, 9)), dma((3, 9)), dma((4,)), dma((4,)), dma((6,)), dma((6,)),
    ]
    return pl.pallas_call(
        kernel,
        name="layer",
        out_shape=jax.ShapeDtypeStruct((ROWS, VD), BF),
        in_specs=[hbm] * 11 + [vmem] * 2 + [pl.BlockSpec(memory_space=pltpu.SMEM)],
        out_specs=vmem,
        scratch_shapes=scratch,
        compiler_params=pltpu.CompilerParams(collective_id=0, has_side_effects=True),
    )(
        query_one, query_two, key_one, key_two, values, resid, out_weight, gate_weight,
        up_weight, down_weight, segments.reshape(1, -1), head_gain.reshape(1, -1),
        mixer_gain.reshape(1, -1), mix_lambda,
    )


def solution(mesh):
    in_specs = (
        P("sp", "tp"), P("sp", "tp"), P("sp", "tp"), P("sp", "tp"), P("sp", "tp"), P("sp", "tp"),
        P("tp"), P("sp"), P(), P(None, "tp"), P("tp"), P("sp", "tp"), P("sp", "tp"), P("tp", "sp"),
    )
    return jax.shard_map(
        body, mesh=mesh, in_specs=in_specs, out_specs=P("sp", "tp"), check_vma=False
    )
```

time: 227 us -> 137 us (0.60)
  the two profiles are of different devices: /device:TPU:256 before, /device:TPU:1 now
where the time goes in v1:
time: 137 us
  Pallas kernels  131 us (96%)
  local copies, waits for them, and re-layouts  4.47 us (3%)
    pallas_call x1, Pallas kernels, body(): pl.pallas_call(kernel, name='layer', out_shape=jax.ShapeDtypeStruct((ROWS...  131 us
    unnamed x4, local copies, waits for them, and re-layouts  3.9 us

profile of v1, /device:TPU:1, one launch (start us, length us, event | category | flops | bytes accessed | tf_op | source)
XLA Modules:
  0.0 136.6 jit_solution(2444605577684838433)
XLA Ops:
  0.7 0.0 copy-start
  0.7 0.7 copy-done
  1.3 0.6 reshape.9.seg_h
  1.9 1.6 %copy.15.down_h = bf16[768,32]{1,0:T(8,128)(2,1)} copy(bf16[768,32]{0,1:T(8,128)(2,1)} %param.27) | data formatting | bytes 98304 | tf_op args[13]
  3.5 131.4 %layer.1 = bf16[384,256]{1,0:T(8,128)(2,1)} custom-call(bf16[384,128]{1,0:T(8,128)(2,1)} %q1_h.1, bf16[384,128]{1,0:T(8,128)(2,1)} %q2_h.1, bf16[384,128]{1,0:T(8,128)(2,1)} %k1_h.1, bf16[384,128]{1,0:T(8,128)(2,1)} %k2_h.1, bf16[384,256]{1,0:T(8,128)(2,1)} %v_h.1, bf16[384,256]{1,0:T(8,128)(2,1)} %resid_h.1, bf16[2048,256]{1,0:T(8,128)(2,1)} %wout_h.1, ...), custom_call_target="tpu_custom_call" | custom-call | tf_op jit(solution)/shard_map/layer/pallas_call | solution.py:444
  135.0 1.6 %copy.18 = bf16[384,256]{1,0:T(8,128)(2,1)} copy(bf16[384,256]{1,0:T(8,128)(2,1)} %layer.1) | data formatting | bytes 393216
Async XLA Ops:
  0.7 0.7 copy-start

commit v2 on v1

v2 whole, which is shorter than its diff:
```python
import functools

import jax
import jax.numpy as jnp
from jax import lax
from jax.experimental import pallas as pl
from jax.experimental.pallas import tpu as pltpu
from jax.sharding import PartitionSpec as P

MESH = pl.DeviceIdType.MESH
BF, F32 = jnp.bfloat16, jnp.float32
ROWS, HD, VD = 384, 128, 256
REACH = 4
BW, AW, GU = 1152, 1152, 768
YM, YP, ZM, ZP = 5, 2, 5, 2
CH, QU = 192, 96
NT = (((1,), (1,)), ((), ()))


def dot(a, b):
    return jnp.dot(a, b, preferred_element_type=F32)


def dot_nt(a, b):
    return lax.dot_general(a, b, NT, preferred_element_type=F32)


def kernel(
    q1_h, q2_h, k1_h, k2_h, v_h, resid_h, wout_h, gate_h, up_h, down_h, seg_h, hg, mg, lam,
    out_ref,
    q1, q2, resid, wout, kbuf, vbuf, gbuf, bbuf, abuf, segq, gains, mref, lref, oacc,
    heads, mids, xn, hid, pown, psend, precv, stage, rhalf, rfull,
    loc, kv_s, kv_r, b1m_s, b1m_r, b1p_s, b1p_r, a1m_s, a1m_r, a1p_s, a1p_r,
    b20_s, b20_r, a20_s, a20_r, b2m_s, b2m_r, b2p_s, b2p_r, a2m_s, a2m_r, a2p_s, a2p_r,
    xg_s, xg_r, d_s, d_r, rs_s, rs_r,
):
    s, t = lax.axis_index("sp"), lax.axis_index("tp")
    z, y = lax.div(s, 8), lax.rem(s, 8)
    x, c = lax.div(t, 2), lax.rem(t, 2)
    o = 1 - c

    def ring(i, by, n):
        return lax.rem(i + (by % n), n)

    yp, ym = {"sp": z * 8 + ring(y, 1, 8)}, {"sp": z * 8 + ring(y, -1, 8)}
    zp, zm = {"sp": ring(z, 1, 8) * 8 + y}, {"sp": ring(z, -1, 8) * 8 + y}
    last, wrap = y == 7, jnp.where(y == 7, REACH, 0)
    turn = {"sp": jnp.where(last, ring(z, 1, 8) * 8 + y, z * 8 + ring(y, 1, 8))}
    xp, xm = {"tp": ring(x, 1, 4) * 2 + c}, {"tp": ring(x, -1, 4) * 2 + c}
    pc = {"tp": x * 2 + o}

    barrier = pltpu.get_barrier_semaphore()
    for dev in (yp, ym, zp, zm, xp, xm, pc):
        pl.semaphore_signal(barrier, inc=1, device_id=dev, device_id_type=MESH)

    loads = [
        (k1_h, kbuf.at[0, :, 0:HD]),
        (k2_h, kbuf.at[0, :, HD : 2 * HD]),
        (v_h, vbuf.at[0]),
        (gate_h, bbuf.at[z, y, :, 0:GU]),
        (up_h, abuf.at[z, y, :, 0:GU]),
        (seg_h, gbuf.at[0, 0]),
        (down_h.at[:, 0 : BW - GU], bbuf.at[z, y, :, GU:BW]),
        (down_h.at[:, BW - GU :], abuf.at[z, y, :, GU:AW]),
        (q1_h, q1),
        (q2_h, q2),
        (resid_h, resid),
        (wout_h, wout),
    ]
    loads = [pltpu.make_async_copy(a, b, loc.at[i]) for i, (a, b) in enumerate(loads)]
    for one in loads:
        one.start()
    gains[t] = jnp.broadcast_to(mg[...], (16, VD))
    for one in loads[:8]:
        one.wait()
    pl.semaphore_wait(barrier, 7)

    pending = []

    def copy(src, dst, ss, rs, dev):
        return pltpu.make_async_remote_copy(
            src_ref=src, dst_ref=dst, send_sem=ss, recv_sem=rs, device_id=dev, device_id_type=MESH
        )

    def send(src, dst, ss, rs, dev):
        one = copy(src, dst, ss, rs, dev)
        one.start()
        pending.append(one)

    def got(ref, ss, rs):
        copy(ref, ref, ss, rs, pc).wait_recv()

    def b_first(which, hop):
        dev, ss, rs, last, step = (
            (ym, b1m_s, b1m_r, YM, 1) if which else (yp, b1p_s, b1p_r, YP, -1)
        )
        shard = y if hop < 0 else ring(y, step * (hop + 1), 8)
        ref = bbuf.at[z, shard]
        if hop >= 0:
            got(ref, ss.at[hop], rs.at[hop])
        if hop + 1 < last:
            send(ref, ref, ss.at[hop + 1], rs.at[hop + 1], dev)
        if hop >= 0 or which:
            copy(ref, ref, b20_s, b20_r, zm).start()

    def a_first(which, hop):
        dev, ss, rs, last, step = (
            (zm, a1m_s, a1m_r, ZM, 1) if which else (zp, a1p_s, a1p_r, ZP, -1)
        )
        shard = z if hop < 0 else ring(z, step * (hop + 1), 8)
        ref = abuf.at[shard, y]
        if hop >= 0:
            got(ref, ss.at[hop], rs.at[hop])
        if hop + 1 < last:
            send(ref, ref, ss.at[hop + 1], rs.at[hop + 1], dev)
        if hop >= 0 or which:
            copy(ref, ref, a20_s, a20_r, ym).start()

    def b_part(row, k):
        return bbuf.at[row, :, :, 0:GU] if k == 0 else bbuf.at[row, :, :, GU:BW]

    def a_part(col, k):
        return abuf.at[:, col, :, 0:GU] if k == 0 else abuf.at[:, col, :, GU:AW]

    def b_second(which, hop, part):
        dev, ss, rs, last, step = (
            (zm, b2m_s, b2m_r, ZM, 1) if which else (zp, b2p_s, b2p_r, ZP, -1)
        )
        row = ring(z, step * (hop + 1), 8)
        if hop == 0 and which:
            got(bbuf.at[row], b20_s, b20_r)
        else:
            got(b_part(row, part), ss.at[hop, part], rs.at[hop, part])
        for k in (0, 1) if hop == 0 and which else (part,):
            if hop + 1 < last:
                ref = b_part(row, k)
                send(ref, ref, ss.at[hop + 1, k], rs.at[hop + 1, k], dev)

    def a_second(which, hop, part):
        dev, ss, rs, last, step = (
            (ym, a2m_s, a2m_r, YM, 1) if which else (yp, a2p_s, a2p_r, YP, -1)
        )
        col = ring(y, step * (hop + 1), 8)
        if hop == 0 and which:
            got(abuf.at[:, col], a20_s, a20_r)
        else:
            got(a_part(col, part), ss.at[hop, part], rs.at[hop, part])
        for k in (0, 1) if hop == 0 and which else (part,):
            if hop + 1 < last:
                ref = a_part(col, k)
                send(ref, ref, ss.at[hop + 1, k], rs.at[hop + 1, k], dev)

    def a_own():
        for k in (0, 1):
            ref = a_part(y, k)
            send(ref, ref, a2p_s.at[0, k], a2p_r.at[0, k], yp)

    def b_own():
        for k in (0, 1):
            ref = b_part(z, k)
            send(ref, ref, b2p_s.at[0, k], b2p_r.at[0, k], zp)

    def kinds(part):
        return ((0, kbuf), (2, gbuf)) if part == 0 else ((1, vbuf),)

    def kv_start(slot, part):
        to = slot + 1 + wrap
        return [
            copy(buf.at[slot], buf.at[to], kv_s.at[i, slot + 1], kv_r.at[i, to], turn)
            for i, buf in kinds(part)
        ]

    def kv_pass(slot, part):
        here = slot + REACH
        return [
            copy(buf.at[here], buf.at[slot], kv_s.at[i, here], kv_r.at[i, slot], yp)
            for i, buf in kinds(part)
        ]

    def kv_got(slot, part):
        for i, buf in kinds(part):
            got(buf.at[slot], kv_s.at[i, slot], kv_r.at[i, slot])

    def kv(slot, part, late):
        @pl.when(y < slot if late else y >= slot)
        def _():
            kv_got(slot, part)
            if slot < REACH:
                for one in kv_start(slot, part):
                    one.start()

    def kv_own(part):
        for one in kv_start(0, part):
            one.start()

    def relay(slot, part):
        @pl.when(last)
        def _():
            kv_got(slot + REACH, part)
            for one in kv_pass(slot, part):
                one.start()

    def kv_done():
        for slot in range(REACH):
            for part in (0, 1):
                for one in kv_start(slot, part):
                    one.wait_send()

        @pl.when(last)
        def _():
            for slot in range(REACH):
                for part in (0, 1):
                    for one in kv_pass(slot + 1, part):
                        one.wait_send()

    def attend(k, first, last):
        ids = gbuf[k].astype(F32) + jnp.where(s >= k, 0.0, 1000.0)

        def chunk(i, carry):
            rows = pl.ds(pl.multiple_of(i * QU, QU), QU)
            same = segq[rows, 0:1] == ids
            if k == 0:
                qpos = i * QU + lax.broadcasted_iota(jnp.int32, (QU, ROWS), 0)
                same = same & (lax.broadcasted_iota(jnp.int32, (QU, ROWS), 1) <= qpos)
            for m, q in enumerate((q1, q2)):
                score = dot_nt(q[rows, :], kbuf[k, :, m * HD : (m + 1) * HD])
                score = jnp.where(same, score * (HD**-0.5 * 1.4426950408889634), -jnp.inf)
                top = jnp.max(score, axis=1, keepdims=True)
                if k > 0:
                    before = mref[m, rows, 0:1]
                    top = jnp.maximum(top, before)
                expo = jnp.exp2(score - top)
                total = jnp.sum(expo, axis=1, keepdims=True)
                value = dot(expo.astype(BF), vbuf[k])
                if k > 0:
                    scale = jnp.exp2(before - top)
                    total = total + scale * lref[m, rows, 0:1]
                    value = value + scale * oacc[m, rows, :]
                mref[m, rows, :] = jnp.broadcast_to(top, (QU, 128))
                lref[m, rows, :] = jnp.broadcast_to(total, (QU, 128))
                oacc[m, rows, :] = value
            return carry

        lax.fori_loop(first, last, chunk, 0)

    def finish_heads(h):
        def chunk(i, carry):
            rows = pl.ds(pl.multiple_of(i * 64, 64), 64)
            head = oacc[0, rows, :] / lref[0, rows, 0:1]
            head = head - lam[0] * (oacc[1, rows, :] / lref[1, rows, 0:1])
            meansq = jnp.mean(head * head, axis=1, keepdims=True)
            heads[t, rows, :] = (head * lax.rsqrt(meansq + 1e-05) * hg[...]).astype(BF)
            return carry

        lax.fori_loop(h * 3, h * 3 + 3, chunk, 0)

    def slot_of(by, core):
        return ring(x, by, 4) * 2 + core

    def x_gather(buf, g, first, n):
        low, high = pl.ds(first, n // 2), pl.ds(first + n // 2, n // 2)
        both = pl.ds(first, n)

        def go(ref, i, dev):
            send(ref, ref, xg_s.at[g, i], xg_r.at[g, i], dev)

        def come(ref, i):
            got(ref, xg_s.at[g, i], xg_r.at[g, i])

        def own():
            mine = buf.at[t, both]
            go(mine, 0, xp)
            go(mine, 1, xm)
            go(mine, 4, pc)

        def near():
            a, b = buf.at[slot_of(-1, c), both], buf.at[slot_of(1, c), both]
            come(a, 0)
            go(buf.at[slot_of(-1, c), low], 2, xp)
            go(a, 5, pc)
            come(b, 1)
            go(buf.at[slot_of(1, c), high], 3, xm)
            go(b, 6, pc)

        def far():
            for i, part in ((2, low), (3, high)):
                ref = buf.at[slot_of(2, c), part]
                come(ref, i)
                go(ref, i + 5, pc)

        def across():
            come(buf.at[slot_of(0, o), both], 4)
            come(buf.at[slot_of(-1, o), both], 5)
            come(buf.at[slot_of(1, o), both], 6)

        def across_far():
            for i, part in ((2, low), (3, high)):
                come(buf.at[slot_of(2, o), part], i + 5)

        return own, near, far, across, across_far

    gain_g = x_gather(gains, 0, 0, 16)
    head_g = [x_gather(heads, 1 + h, h * CH, CH) for h in (0, 1)]
    mid_g = [x_gather(mids, 3 + h, h * CH, CH) for h in (0, 1)]

    def project(h, slots, first):
        rows = pl.ds(h * CH, CH)
        total = None if first else oacc[0, rows, :]
        for by, core in slots:
            i = slot_of(by, core)
            w = wout[pl.ds(pl.multiple_of(i * VD, VD), VD), :]
            part = dot(heads[i, rows, :], w)
            total = part if total is None else total + part
        return rows, total

    def project_near(h):
        slots = ((0, c), (-1, c), (1, c), (0, o), (-1, o), (1, o))
        rows, total = project(h, slots, True)
        oacc[0, rows, :] = total

    def project_far(h):
        rows, total = project(h, ((2, c), (2, o)), False)
        mids[t, rows, :] = (resid[rows, :].astype(F32) + total).astype(BF)

    def normalise(h):
        def chunk(i, carry):
            rows = pl.ds(pl.multiple_of(i * 32, 32), 32)
            mid = [mids[j, rows, :].astype(F32) for j in range(8)]
            squares = sum([m * m for m in mid])
            meansq = jnp.sum(squares, axis=1, keepdims=True) * (1.0 / (8 * VD))
            scale = lax.rsqrt(meansq + 1e-06)
            for j in range(8):
                gain = gains[j][0:1, :]
                xn[rows, j * VD : (j + 1) * VD] = (mid[j] * scale * gain).astype(BF)
            return carry

        lax.fori_loop(h * 6, h * 6 + 6, chunk, 0)

    def hidden(h):
        rows = pl.ds(h * CH, CH)

        def tile(i, carry):
            cols = pl.ds(pl.multiple_of(i * 256, 256), 256)
            gate = dot(xn[rows, :], bbuf[:, :, :, cols].reshape(2048, 256))
            up = dot(xn[rows, :], abuf[:, :, :, cols].reshape(2048, 256))
            hid[rows, cols] = (gate / (1.0 + jnp.exp(-gate)) * up).astype(BF)
            return carry

        lax.fori_loop(0, 3, tile, 0)

    def terms(i, core):
        i = slot_of((2, 1, -1, 0)[i], core)
        one = dot_nt(hid[:, 0 : BW - GU], bbuf[i, :, :, GU:BW].reshape(VD, BW - GU))
        two = dot_nt(hid[:, BW - GU :], abuf[i, :, :, GU:AW].reshape(VD, AW - GU))
        return one + two

    low, high = pl.ds(0, CH), pl.ds(CH, CH)

    def down(i):
        psend[i] = terms(i, o).astype(BF)
        send(psend.at[i], precv.at[i], d_s.at[i], d_r.at[i], pc)
        pown[i] = terms(i, c)

    def cross(i):
        got(precv.at[i], d_s.at[i], d_r.at[i])

    def chip_sum(i, part):
        return pown[i, part, :] + precv[i, part, :].astype(F32)

    def go(i, part, value, to, k, dev):
        stage[i, part, :] = value.astype(BF)
        send(stage.at[i, part], to.at[part], rs_s.at[k], rs_r.at[k], dev)

    def come(ref, part, k):
        got(ref.at[part], rs_s.at[k], rs_r.at[k])

    def sum_0():
        cross(0)
        go(0, low, chip_sum(0, low), rhalf, 0, xp)
        go(0, high, chip_sum(0, high), rhalf, 1, xm)

    def sum_1():
        cross(1)
        go(1, high, chip_sum(1, high), rfull.at[0], 2, xp)

    def sum_2():
        cross(2)
        go(2, low, chip_sum(2, low), rfull.at[1], 3, xm)

    def sum_3():
        come(rhalf, low, 0)
        go(1, low, chip_sum(1, low) + rhalf[low, :].astype(F32), rfull.at[0], 4, xp)
        come(rhalf, high, 1)
        go(2, high, chip_sum(2, high) + rhalf[high, :].astype(F32), rfull.at[1], 5, xm)

    def sum_4():
        cross(3)
        pown[3] = pown[3] + precv[3].astype(F32) + mids[t].astype(F32)
        for part, i, k in ((high, 0, 2), (low, 1, 3)):
            come(rfull.at[i], part, k)
            pown[3, part, :] += rfull[i, part, :].astype(F32)
        for part, i, k in ((low, 0, 4), (high, 1, 5)):
            come(rfull.at[i], part, k)
            out_ref[part, :] = (pown[3, part, :] + rfull[i, part, :].astype(F32)).astype(BF)

    events = []

    def at(time, what, *args):
        events.append((time, len(events), what, args))

    for which, first in ((True, b_first), (True, a_first)):
        for hop, time in enumerate((3.4, 6.7, 11.4, 16.2, 19.5)):
            at(time, first, True, hop)
    for first in (b_first, a_first):
        at(3.5, first, False, 0)
        at(9.2 if first is b_first else 6.8, first, False, 1)
    at(2.0, gain_g[0])
    at(7.5, gain_g[1])
    at(11.0, gain_g[2])
    at(11.5, gain_g[3])
    at(14.5, gain_g[4])
    at(2.1, attend, 0, 0, 4)
    at(3.6, kv_own, 1)
    for slot, (tk, tv) in enumerate(((9.0, 14.0), (18.4, 22.6), (26.8, 31.0), (35.2, 39.4))):
        for part, time in enumerate((tk, tv)):
            at(time, relay, slot + 1, part)
            at(time, kv, slot + 1, part, False)
        at(tk + 6.5, kv, slot + 1, 0, True)
        at(tv + 6.5, kv, slot + 1, 1, True)
        if slot < 3:
            at(tv + 6.6, attend, slot + 1, 0, 4)
    at(39.5, a_own)
    at(31.2, b_own)
    for second in (a_second, b_second):
        times = ((23.0, 23.0), (32.75, 37.0), (45.0, 49.5), (57.5, 61.0), (73.0, 77.5))
        for hop, pair in enumerate(times):
            for part in (0,) if hop == 0 else (0, 1):
                at(pair[part], second, True, hop, part)
    for hop, pair in enumerate(((53.0, 57.0), (66.0, 70.0))):
        for part in (0, 1):
            at(pair[part], a_second, False, hop, part)
    for hop, pair in enumerate(((45.5, 50.0), (60.0, 64.0))):
        for part in (0, 1):
            at(pair[part], b_second, False, hop, part)
    for h, late in ((0, 7.5), (1, 9.5)):
        at(38.7 + late, attend, REACH, 2 * h, 2 * h + 2)
        at(38.8 + late, finish_heads, h)
        at(38.9 + late, head_g[h][0])
        at(43.0 + late, head_g[h][1])
        at(44.8 + late, head_g[h][3])
        at(44.9 + late, project_near, h)
        at(46.0 + late, head_g[h][2])
        at(47.4 + late, head_g[h][4])
        at(47.5 + late, project_far, h)
        at(47.6 + late, mid_g[h][0])
        at(51.8 + late, mid_g[h][1])
        at(54.8 + late, mid_g[h][2])
        at(56.0 + late, mid_g[h][3])
        at(56.1 + late, mid_g[h][4])
        at(56.2 + late, normalise, h)

    def drain():
        while pending:
            pending.pop(0).wait_send()
        kv_done()
        copy(bbuf.at[z], bbuf.at[z], b20_s, b20_r, zm).wait_send()
        copy(abuf.at[:, y], abuf.at[:, y], a20_s, a20_r, ym).wait_send()

    at(72.9, drain)
    at(74.0, hidden, 0)
    at(74.1, hidden, 1)
    tail = (
        (down, 0), (down, 1), (sum_0,), (down, 2), (sum_1,), (down, 3), (sum_2,), (sum_3,), (sum_4,)
    )
    for i, one in enumerate(tail):
        at(78.0 + i, *one)

    b_first(True, -1)
    b_first(False, -1)
    a_first(True, -1)
    a_first(False, -1)
    kv_own(0)
    for one in loads[8:]:
        one.wait()
    ids = jnp.broadcast_to(gbuf[0].astype(F32), (128, ROWS))
    segq[...] = ids.T
    for _, _, what, args in sorted(events, key=lambda e: e[:2]):
        what(*args)

    for one in pending:
        one.wait_send()


def body(
    resid, query_one, key_one, query_two, key_two, values, mix_lambda, segments, head_gain,
    out_weight, mixer_gain, gate_weight, up_weight, down_weight,
):
    hbm = pl.BlockSpec(memory_space=pltpu.HBM)
    vmem = pl.BlockSpec(memory_space=pltpu.VMEM)
    dma = pltpu.SemaphoreType.DMA
    scratch = [
        pltpu.VMEM((ROWS, HD), BF), pltpu.VMEM((ROWS, HD), BF), pltpu.VMEM((ROWS, VD), BF),
        pltpu.VMEM((2048, VD), BF),
        pltpu.VMEM((9, ROWS, 2 * HD), BF), pltpu.VMEM((9, ROWS, VD), BF),
        pltpu.VMEM((9, 1, ROWS), jnp.int32),
        pltpu.VMEM((8, 8, 32, BW), BF), pltpu.VMEM((8, 8, 32, AW), BF),
        pltpu.VMEM((ROWS, 128), F32), pltpu.VMEM((8, 16, VD), F32),
        pltpu.VMEM((2, ROWS, 128), F32), pltpu.VMEM((2, ROWS, 128), F32),
        pltpu.VMEM((2, ROWS, VD), F32),
        pltpu.VMEM((8, ROWS, VD), BF), pltpu.VMEM((8, ROWS, VD), BF),
        pltpu.VMEM((ROWS, 2048), BF), pltpu.VMEM((ROWS, 768), BF),
        pltpu.VMEM((4, ROWS, VD), F32), pltpu.VMEM((4, ROWS, VD), BF),
        pltpu.VMEM((4, ROWS, VD), BF), pltpu.VMEM((3, ROWS, VD), BF),
        pltpu.VMEM((ROWS, VD), BF), pltpu.VMEM((2, ROWS, VD), BF),
        dma((12,)), dma((3, 9)), dma((3, 9)),
        dma((YM,)), dma((YM,)), dma((YP,)), dma((YP,)),
        dma((ZM,)), dma((ZM,)), dma((ZP,)), dma((ZP,)),
        dma, dma, dma, dma,
        dma((ZM, 2)), dma((ZM, 2)), dma((ZP, 2)), dma((ZP, 2)),
        dma((YM, 2)), dma((YM, 2)), dma((YP, 2)), dma((YP, 2)),
        dma((5, 9)), dma((5, 9)), dma((4,)), dma((4,)), dma((6,)), dma((6,)),
    ]
    return pl.pallas_call(
        kernel,
        name="layer",
        out_shape=jax.ShapeDtypeStruct((ROWS, VD), BF),
        in_specs=[hbm] * 11 + [vmem] * 2 + [pl.BlockSpec(memory_space=pltpu.SMEM)],
        out_specs=vmem,
        scratch_shapes=scratch,
        compiler_params=pltpu.CompilerParams(collective_id=0, has_side_effects=True),
    )(
        query_one, query_two, key_one, key_two, values, resid, out_weight, gate_weight,
        up_weight, down_weight.T, segments, head_gain.reshape(1, -1),
        mixer_gain.reshape(1, -1), mix_lambda,
    )


def solution(mesh):
    in_specs = (
        P("sp", "tp"), P("sp", "tp"), P("sp", "tp"), P("sp", "tp"), P("sp", "tp"), P("sp", "tp"),
        P("tp"), P("sp"), P(), P(None, "tp"), P("tp"), P("sp", "tp"), P("sp", "tp"), P("tp", "sp"),
    )
    return jax.shard_map(
        body, mesh=mesh, in_specs=in_specs, out_specs=P("sp", "tp"), check_vma=False
    )
```

time: 137 us -> 111 us (0.81)
  Pallas kernels: 131 us -> 109 us
  local copies, waits for them, and re-layouts: 4.47 us -> 1.62 us
    pallas_call x1, Pallas kernels: 131 us -> 109 us  [body(): pl.pallas_call(kernel, name='layer', out_shape=jax.ShapeDtypeStruct((ROWS...]
    unnamed x4 -> x1, local copies, waits for them, and re-layouts: 3.9 us -> 1.62 us
where the time goes in v2:
time: 111 us
  Pallas kernels  109 us (98%)
  local copies, waits for them, and re-layouts  1.62 us (1%)
    pallas_call x1, Pallas kernels, body(): pl.pallas_call(kernel, name='layer', out_shape=jax.ShapeDtypeStruct((ROWS...  109 us

profile of v2, /device:TPU:1, one launch (start us, length us, event | category | flops | bytes accessed | tf_op | source)
XLA Modules:
  0.0 111.2 jit_solution(14958434399076999768)
XLA Ops:
  0.7 109.0 %layer.1 = bf16[384,256]{1,0:T(8,128)(2,1)} custom-call(bf16[384,128]{1,0:T(8,128)(2,1)} %q1_h.1, bf16[384,128]{1,0:T(8,128)(2,1)} %q2_h.1, bf16[384,128]{1,0:T(8,128)(2,1)} %k1_h.1, bf16[384,128]{1,0:T(8,128)(2,1)} %k2_h.1, bf16[384,256]{1,0:T(8,128)(2,1)} %v_h.1, bf16[384,256]{1,0:T(8,128)(2,1)} %resid_h.1, bf16[2048,256]{1,0:T(8,128)(2,1)} %wout_h.1, ...), custom_call_target="tpu_custom_call" | custom-call | tf_op jit(solution)/shard_map/layer/pallas_call | solution.py:523
  109.6 1.6 %copy.17 = bf16[384,256]{1,0:T(8,128)(2,1)} copy(bf16[384,256]{1,0:T(8,128)(2,1)} %layer.1) | data formatting | bytes 393216
